TPU v7x, 256 devices: a 4x2x16 block of a 4x16x16 slice. The times are simulated.
256 devices in a mesh: grp: 2 (over y), sp: 32 (over z, core), tp: 4 (over x).
Axes of the slice: x: 4, y: 2, z: 16, core: 2. Of those that a mesh axis runs over, the one named last changes fastest.
The devices are a block of a 4x16x16 slice.
Arguments:
- residual: bfloat16 [16384, 2048], P(('grp', 'sp', 'tp')), parts along dimension 0, may hold values from -6 to 6
- query_nope: bfloat16 [16384, 1024], P(('grp', 'sp'), 'tp'), parts along dimension 0, may hold values from -6 to 6
- query_rope: bfloat16 [16384, 512], P(('grp', 'sp'), 'tp'), parts along dimension 0, may hold values from -240 to 240
- kv_latent: bfloat16 [16384, 256], P(('grp', 'sp')), parts along dimension 0, may hold values from -6 to 6
- rope_key: bfloat16 [16384, 64], P(('grp', 'sp')), parts along dimension 0, may hold values from -6 to 6
- latent_gain: float32 [256], replicated, may hold values from 0.1 to 1.9
- w_key: bfloat16 [256, 1024], P(None, 'tp'), may hold values from -0.375 to 0.375
- w_value: bfloat16 [256, 1024], P(None, 'tp'), may hold values from -0.375 to 0.375
- w_out: bfloat16 [1024, 2048], P('tp'), may hold values from -0.1875 to 0.1875
- post_gain: float32 [2048], replicated, may hold values from 0.1 to 1.9
- routes: int32 [16384, 2], P(('grp', 'sp', 'tp')), parts along dimension 0, may hold values from 0 to 31, all different within a row; in each aligned block of 64 rows (0 to 63, 64 to 127, ...) at most 6 rows name the same one
- route_weight: float32 [16384, 2], P(('grp', 'sp', 'tp')), parts along dimension 0, may hold values from 0.25 to 1
- moe_gain: float32 [2048], replicated, may hold values from 0.1 to 1.9
- w_gate: bfloat16 [32, 2048, 3584], P('sp', None, 'tp'), may hold values from -0.125 to 0.125
- w_up: bfloat16 [32, 2048, 3584], P('sp', None, 'tp'), may hold values from -0.125 to 0.125
- w_down: bfloat16 [32, 3584, 2048], P('sp', 'tp'), may hold values from -0.09375 to 0.09375
Outputs:
- mixed: bfloat16 [16384, 2048], P(('grp', 'sp', 'tp')), parts along dimension 0
There are 2 independent parts, one for each index of `grp`. A program takes and returns all parts, laid end to end along the dimension named above; an argument that names none is the same for every part. Nothing has to cross between parts.
Inputs may be any that keep to these rules, and one draw needn't show every extreme that they name: `routes`: each row names two different experts. Among the 64 rows of one device no expert is named more than 6 times, and some device names some expert exactly 6 times.
All inputs are finite; a program needn't handle non-finite values.
Results may differ from a plain program's by a relative error of at most 0.014.
Values may be sent and summed in bfloat16 or wider, within the bound.
A program may use at most 128 MiB of HBM per device.

v0:
```python
import jax
import jax.numpy as jnp
from jax import lax
from jax.sharding import Mesh
from jax.sharding import PartitionSpec as P

HEADS = 8
NOPE = 128
ROPE = 64
VDIM = 128
SP = ("sp_0", "sp_1")
GRP_SP_TP = ("grp", "sp_0", "sp_1", "tp")
GRP_SP = ("grp", "sp_0", "sp_1")


epsilon = 1e-06
rope_base = 10000.0


def side_by_side(arrays, axis, dim, along):
    widths = [a.shape[along] for a in arrays]
    both = jnp.concatenate(arrays, axis=along)
    result = lax.all_gather(both, axis, axis=dim, tiled=True)
    return tuple(jnp.split(result, [sum(widths[:k]) for k in range(1, len(widths))], axis=along))


def split_up(array, dim, length):
    before, after = (array.shape[:dim], array.shape[dim + 1 :])
    return jnp.moveaxis(array.reshape(*before, length, -1, *after), dim, 0)


def summed_on_arrival(array, axis, dim):
    length = lax.axis_size(axis)
    pieces = lax.all_to_all(split_up(array, dim, length), axis, 0, 0, tiled=True)
    return jnp.sum(pieces.astype(jnp.float32), axis=0)


def in_order(pieces, dim):
    dims = list(pieces.shape[1:])
    dims[dim] *= pieces.shape[0]
    return jnp.moveaxis(pieces, 0, dim).reshape(dims)


def exchange_in_order(pieces, axes, order):
    inside = pieces.shape[1:]
    result = pieces.reshape(*(lax.axis_size(a) for a in axes), *inside)
    for k in order:
        result = lax.all_to_all(result, axes[k], k, k, tiled=True)
    return result.reshape(-1, *inside)


def two_step_exchange(array, groups, order, split_dim, concat_dim):
    length = lax.axis_size(groups[0]) * lax.axis_size(groups[1])
    pieces = split_up(array, split_dim, length)
    return in_order(exchange_in_order(pieces, groups, order), concat_dim)


def rms_scale(inputs, gain_vector):
    mean_square = jnp.mean(inputs * inputs, axis=-1, keepdims=True)
    return inputs * lax.rsqrt(mean_square + epsilon) * gain_vector


def tables(positions, rot_width):
    frequency = 1.0 / rope_base ** (jnp.arange(0, rot_width, 2, dtype=jnp.float32) / rot_width)
    angles = positions.astype(jnp.float32)[:, None] * frequency[None, :]
    return (jnp.cos(angles), jnp.sin(angles))


def rotate(inputs, cosine_table, sine_table):
    half_width = inputs.shape[-1] // 2
    first_half = inputs[..., :half_width]
    second_half = inputs[..., half_width:]
    return jnp.concatenate(
        [
            first_half * cosine_table - second_half * sine_table,
            second_half * cosine_table + first_half * sine_table,
        ],
        axis=-1,
    )


def expand(latent_rows, rope_rows, latent_gain, w_key, w_value):
    normed = rms_scale(latent_rows.astype(jnp.float32), latent_gain).astype(jnp.bfloat16)
    key_plain = jnp.dot(normed, w_key, preferred_element_type=jnp.float32).astype(jnp.bfloat16)
    value_plain = jnp.dot(normed, w_value, preferred_element_type=jnp.float32).astype(jnp.bfloat16)
    key_positions = jnp.arange(latent_rows.shape[0], dtype=jnp.int32)
    cosine_table, sine_table = tables(key_positions, rope_rows.shape[1])
    key_turned = rotate(rope_rows.astype(jnp.float32), cosine_table, sine_table).astype(
        jnp.bfloat16
    )
    return (key_plain, value_plain, key_turned)


def body(
    residual,
    query_nope,
    query_rope,
    kv_latent,
    rope_key,
    latent_gain,
    w_key,
    w_value,
    w_out,
    post_gain,
    routes,
    route_weight,
    moe_gain,
    w_gate,
    w_up,
    w_down,
):
    tok_rows = query_nope.shape[0]
    heads_here = HEADS // lax.axis_size("tp")
    first_row = lax.axis_index(SP) * tok_rows
    last_row = first_row + tok_rows - 1
    positions = first_row + jnp.arange(tok_rows, dtype=jnp.int32)
    cosine_table, sine_table = tables(positions, ROPE)
    query_plain = query_nope.reshape(tok_rows, heads_here, NOPE)
    query_turned = rotate(
        query_rope.reshape(tok_rows, heads_here, ROPE).astype(jnp.float32),
        cosine_table[:, None, :],
        sine_table[:, None, :],
    ).astype(jnp.bfloat16)
    score_scale = (NOPE + ROPE) ** (-0.5)

    def update(state_now, key_plain, value_plain, key_turned):
        row_max, row_sum, running = state_now
        key_count = key_plain.shape[0]
        key_heads = key_plain.reshape(key_count, heads_here, NOPE)
        value_heads = value_plain.reshape(key_count, heads_here, VDIM)
        scores = jnp.einsum(
            "thd,shd->hts", query_plain, key_heads, preferred_element_type=jnp.float32
        )
        scores = (
            scores
            + jnp.einsum(
                "thd,sd->hts", query_turned, key_turned, preferred_element_type=jnp.float32
            )
        ) * score_scale
        key_positions = jnp.arange(key_count, dtype=jnp.int32)
        allowed = key_positions[None, :] <= positions[:, None]
        scores = jnp.where(allowed[None], scores, -1e30)
        new_max = jnp.maximum(row_max, jnp.max(scores, axis=-1))
        weights = jnp.exp(scores - new_max[..., None])
        row_sum = jnp.sum(weights, axis=-1)
        running = jnp.einsum(
            "hts,shd->htd",
            weights.astype(jnp.bfloat16),
            value_heads,
            preferred_element_type=jnp.float32,
        )
        return (new_max, row_sum, running)

    start_state = (
        jnp.full((heads_here, tok_rows), -1e30, jnp.float32),
        jnp.zeros((heads_here, tok_rows), jnp.float32),
        jnp.zeros((heads_here, tok_rows, VDIM), jnp.float32),
    )
    pieces = side_by_side((kv_latent, rope_key), SP, 0, 1)

    def take_piece(state_in):
        key_plain, value_plain, key_turned = expand(
            pieces[0], pieces[1], latent_gain, w_key, w_value
        )
        return update(state_in, key_plain, value_plain, key_turned)

    def skip_piece(state_in):
        return state_in

    final_state = lax.cond(jnp.int32(0) <= last_row, take_piece, skip_piece, start_state)
    attended = (final_state[2] / final_state[1][..., None]).transpose(1, 0, 2)
    attended = attended.reshape(tok_rows, heads_here * VDIM).astype(jnp.bfloat16)
    chosen = attended
    product = jnp.dot(chosen, w_out, preferred_element_type=jnp.float32)
    branch = summed_on_arrival(
        product.astype(jnp.bfloat16).astype(jnp.float32).astype(jnp.bfloat16), "tp", 0
    )
    updated = (residual.astype(jnp.float32) + rms_scale(branch, post_gain)).astype(jnp.bfloat16)
    moe_in = rms_scale(updated.astype(jnp.float32), moe_gain).astype(jnp.bfloat16)
    token_count = routes.shape[0]
    experts = lax.axis_size(SP)
    capacity = max(2, 3 * token_count // experts)
    onehot = (routes[:, :, None] == jnp.arange(experts, dtype=jnp.int32)[None, None, :]).astype(
        jnp.int32
    )
    flat_hits = onehot.reshape(token_count * 2, experts)
    order_in = jnp.cumsum(flat_hits, axis=0) - flat_hits
    slot_ids = jnp.sum(
        (order_in + jnp.arange(experts, dtype=jnp.int32)[None, :] * capacity) * flat_hits, axis=1
    )
    placing = slot_ids[:, None] == jnp.arange(experts * capacity, dtype=jnp.int32)[None, :]
    placing = placing.astype(jnp.bfloat16).reshape(token_count, 2, experts * capacity)
    sending = jnp.einsum("tks,td->sd", placing, moe_in, preferred_element_type=jnp.float32).astype(
        jnp.bfloat16
    )
    received = two_step_exchange(sending, ("sp_0", "sp_1"), (1, 0), 0, 0)
    span_rows = lax.all_gather(received, "tp", axis=0, tiled=True)
    gate_pre = jnp.dot(span_rows, w_gate[0], preferred_element_type=jnp.float32)
    up_proj = jnp.dot(span_rows, w_up[0], preferred_element_type=jnp.float32)
    hidden_rows = (jax.nn.silu(gate_pre) * up_proj).astype(jnp.bfloat16)
    chosen = hidden_rows
    product = jnp.dot(chosen, w_down[0], preferred_element_type=jnp.float32)
    expert_out = summed_on_arrival(
        product.astype(jnp.bfloat16).astype(jnp.float32).astype(jnp.bfloat16), "tp", 0
    ).astype(jnp.bfloat16)
    returned = two_step_exchange(expert_out, ("sp_0", "sp_1"), (1, 0), 0, 0)
    gathered_back = jnp.einsum("tks,sd->tkd", placing, returned, preferred_element_type=jnp.float32)
    weighted = jnp.sum(gathered_back * route_weight[:, :, None], axis=1)
    return (updated.astype(jnp.float32) + weighted).astype(jnp.bfloat16)


def solution(mesh):
    torus = Mesh(
        mesh.devices.reshape(mesh.shape["grp"], 16, 2, mesh.shape["tp"]),
        ("grp", "sp_0", "sp_1", "tp"),
    )
    placed = (
        P(GRP_SP_TP, None),
        P(GRP_SP, "tp"),
        P(GRP_SP, "tp"),
        P(GRP_SP, None),
        P(GRP_SP, None),
        P(),
        P(None, "tp"),
        P(None, "tp"),
        P("tp", None),
        P(),
        P(GRP_SP_TP, None),
        P(GRP_SP_TP, None),
        P(),
        P(SP, None, "tp"),
        P(SP, None, "tp"),
        P(SP, "tp", None),
    )
    return jax.shard_map(
        body, mesh=torus, in_specs=placed, out_specs=P(GRP_SP_TP, None), check_vma=False
    )
```

profile of v0, /device:TPU:40, one launch (start us, length us, event | category | flops | bytes accessed | tf_op | source)
XLA Modules:
  0.0 406.6 jit_solution(10510677321278599137)
XLA Ops:
  6.6 1.1 copy.57
  7.6 1.4 pad_maximum_fusion
  9.2 0.9 copy.58
  10.1 0.2 multiply_cosine_fusion.1
  10.4 94.3 %all-gather.3.cloned.1.call-done = bf16[8192,320]{0,1:T(8,128)(2,1)} async-done(((bf16[256,320]{0,1:T(8,128)(2,1)}), bf16[8192,320]{0,1:T(8,128)(2,1)}) %all-gather.3.cloned.1.call-update) | async-done | bytes 5242896 | tf_op jit(solution)/shard_map/all_gather | solution.py:23
  104.7 51.3 %conditional.1 = (f32[2,256]{1,0:T(2,128)S(1)}, f32[2,256,128]{1,2,0:T(8,128)S(1)}) conditional(s32[]{:T(128)} %convert_element_type.107, () %tuple.13, (s32[]{:T(128)}, s32[256]{0:T(256)S(1)}, bf16[8192,320]{0,1:T(8,128)(2,1)}, f32[256]{0:T(256)}, bf16[256,256]{1,0:T(8,128)(2,1)}, /*index=5*/bf16[256,256]{1,0:T(8,128)(2,1)}, ...), branch_computations={%region_0.0_spmd, %region_1.5_spmd} | conditional | flops 4899749888 | bytes 194434480 | solution.py:170
  104.7 3.1 fusion.4
  107.8 3.7 convolution_convert_fusion.1
  111.5 8.1 %fusion.22 = f32[2,8192,256]{2,1,0:T(8,128)} fusion(bf16[8192,2,128]{0,2,1:T(8,128)(2,1)S(1)} %bitcast.57, bf16[256,256]{1,0:T(8,128)(2,1)S(1)} %copy-done.3), kind=kOutput, calls=%fused_computation.30 | convolution fusion | flops 1073741824 | bytes 21102592 | tf_op jit(solution)/shard_map/cond/branch_1_fun/thd,shd->hts/dot_general | solution.py:131
  119.6 1.4 slice_convert_fusion
  121.0 4.4 %fusion.15 = (bf16[8192,32]{0,1:T(8,128)(2,1)S(1)}, bf16[8192,32]{0,1:T(8,128)(2,1)S(1)}) fusion(f32[8192,64]{0,1:T(8,128)S(1)} %slice_convert_fusion, f32[32]{0:T(128)S(1)} %negate_power_fusion, f32[8192]{0:T(1024)S(1)} %iota_convert_fusion), kind=kLoop, calls=%fused_computation.23 | loop fusion | flops 2359296 | bytes 3178624 | tf_op jit(solution)/shard_map/convert.1
  125.4 1.4 iota_compare_fusion
  126.8 11.0 %fusion.53 = (f32[2,256]{1,0:T(2,128)S(1)}, f32[2,256,8192]{1,2,0:T(8,128)}) fusion(bf16[256,2,64]{0,2,1:T(8,128)(2,1)S(1)} %get-tuple-element.33, bf16[8192,32]{0,1:T(8,128)(2,1)S(1)} %get-tuple-element.51, bf16[8192,32]{0,1:T(8,128)(2,1)S(1)} %get-tuple-element.50, f32[2,8192,256]{2,1,0:T(8,128)} %fusion.22, pred[256,8192]{0,1:T(8,128)(4,1)S(1)} %iota_compare_fusion), kind=kOutput, calls=%fused_computation.85 | convolution fusion | flops 555744768 | bytes 36767744 | tf_op jit(solution)/shard_map/cond/branch_1_fun/thd,sd->hts/dot_general | solution.py:136
  137.9 3.8 convolution_convert_fusion
  141.6 3.2 copy-done.1
  144.9 3.1 fusion.7
  148.0 8.0 %fusion.3 = f32[2,256]{1,0:T(2,128)S(1)} fusion(f32[2,256,8192]{1,2,0:T(8,128)} %get-tuple-element.53, f32[2,256]{1,0:T(2,128)S(1)} %broadcast_maximum_fusion), kind=kLoop, calls=%fused_computation.5 | loop fusion | flops 8388096 | bytes 16781312 | tf_op jit(solution)/shard_map/cond/branch_1_fun/reduce_sum | solution.py:145
  156.1 1.5 convolution_convert_fusion.2
  157.5 4.2 %all-to-all-start = ((bf16[4,64,2048]{2,1,0:T(8,128)(2,1)}), bf16[4,64,2048]{2,1,0:T(8,128)(2,1)S(1)}, u32[]{:S(2)}, u32[]{:S(2)}) async-start(bf16[4,64,2048]{2,1,0:T(8,128)(2,1)} %bitcast.8), calls=%async_computation | async-start | bytes 2097152 | tf_op jit(solution)/shard_map/all_to_all | solution.py:34
  162.1 0.2 reduce_window_sum.11
  162.2 0.2 select_reduce_fusion
  162.4 0.1 eq.58
  162.8 14.5 %all-to-all-done = bf16[4,64,2048]{2,1,0:T(8,128)(2,1)S(1)} async-done(((bf16[4,64,2048]{2,1,0:T(8,128)(2,1)}), bf16[4,64,2048]{2,1,0:T(8,128)(2,1)S(1)}, u32[]{:S(2)}, u32[]{:S(2)}) %all-to-all-start) | async-done | bytes 1048608 | tf_op jit(solution)/shard_map/all_to_all | solution.py:34
  177.2 0.2 convert_reduce_fusion
  177.4 0.1 multiply_reduce_fusion
  177.5 0.3 fusion.40
  177.8 0.4 convolution_convert_fusion.3
  178.3 0.3 reshape_reshape.12
  178.5 0.4 copy.63
  179.0 4.4 %all_to_all.30 = bf16[16,2,6,2048]{3,0,2,1:T(8,128)(2,1)S(1)} all-to-all(bf16[16,2,6,2048]{3,0,2,1:T(8,128)(2,1)S(1)} %copy.63), channel_id=1, replica_groups=mesh['grp'=2,'sp_0'=16,'sp_1'=2,'tp'=4] {'sp_1'}, dimensions={1} | all-to-all | bytes 1572864 | tf_op jit(solution)/shard_map/all_to_all | solution.py:48
  183.4 0.8 copy.64
  184.2 48.8 %all_to_all.31 = bf16[16,2,6,2048]{3,1,2,0:T(2,128)(2,1)S(1)} all-to-all(bf16[16,2,6,2048]{3,1,2,0:T(2,128)(2,1)S(1)} %copy.64), channel_id=1, replica_groups=mesh['grp'=2,'sp_0'=16,'sp_1'=2,'tp'=4] {'sp_0'}, dimensions={0} | all-to-all | bytes 1572864 | tf_op jit(solution)/shard_map/all_to_all | solution.py:48
  232.9 0.3 copy.65
  233.3 1.1 reshape_reshape.13
  234.5 38.4 %all-gather.5.cloned.1.call-done = bf16[768,2048]{1,0:T(8,128)(2,1)} async-done(((bf16[192,2048]{1,0:T(8,128)(2,1)}), bf16[768,2048]{1,0:T(8,128)(2,1)}) %all-gather.5.cloned.1.call-update) | async-done | bytes 3145744 | tf_op jit(solution)/shard_map/all_gather | solution.py:197
  272.9 8.0 %fusion.28 = f32[768,896]{1,0:T(8,128)} fusion(bf16[768,2048]{1,0:T(8,128)(2,1)} %all-gather.5.cloned.1.call-done, bf16[1,2048,896]{2,1,0:T(8,128)(2,1)} %param.32), kind=kOutput, calls=%fused_computation.41 | convolution fusion | flops 2818572288 | bytes 9568256 | tf_op jit(solution)/shard_map/dot_general | solution.py:199
  280.9 12.2 %fusion.32 = bf16[768,2048]{1,0:T(8,128)(2,1)} fusion(bf16[1,896,2048]{2,1,0:T(8,128)(2,1)} %param.33, f32[768,896]{1,0:T(8,128)} %fusion.28, bf16[768,2048]{1,0:T(8,128)(2,1)} %all-gather.5.cloned.1.call-done, bf16[1,2048,896]{2,1,0:T(8,128)(2,1)} %param.31), kind=kOutput, calls=%fused_computation.45 | convolution fusion | flops 5642846208 | bytes 16384000 | tf_op jit(solution)/shard_map/dot_general | solution.py:202
  293.0 43.0 %all_to_all.32 = bf16[4,192,2048]{2,1,0:T(8,128)(2,1)} all-to-all(bf16[4,192,2048]{2,1,0:T(8,128)(2,1)} %bitcast.59), channel_id=1, replica_groups=mesh['grp'=2,'sp_0'=16,'sp_1'=2,'tp'=4] {'tp'}, dimensions={0} | all-to-all | bytes 6291456 | tf_op jit(solution)/shard_map/all_to_all | solution.py:34
  336.1 2.6 reduce_sum.89
  338.6 0.3 reshape_reshape.14
  338.9 0.4 copy.66
  339.3 4.4 %all_to_all.33 = bf16[16,2,6,2048]{3,0,2,1:T(8,128)(2,1)S(1)} all-to-all(bf16[16,2,6,2048]{3,0,2,1:T(8,128)(2,1)S(1)} %copy.66), channel_id=1, replica_groups=mesh['grp'=2,'sp_0'=16,'sp_1'=2,'tp'=4] {'sp_1'}, dimensions={1} | all-to-all | bytes 1572864 | tf_op jit(solution)/shard_map/all_to_all | solution.py:48
  343.7 0.8 copy.67
  344.5 53.5 %all_to_all.34 = bf16[16,2,6,2048]{3,1,2,0:T(2,128)(2,1)S(1)} all-to-all(bf16[16,2,6,2048]{3,1,2,0:T(2,128)(2,1)S(1)} %copy.67), channel_id=1, replica_groups=mesh['grp'=2,'sp_0'=16,'sp_1'=2,'tp'=4] {'sp_0'}, dimensions={0} | all-to-all | bytes 1572864 | tf_op jit(solution)/shard_map/all_to_all | solution.py:48
  398.1 0.3 copy.68
  398.4 0.3 reshape.183
  398.7 0.4 fusion.37
  399.0 0.8 fusion.43
  (44 shorter events, 0.8 us)
Async XLA Ops:
  6.5 149.5 %copy-start = (bf16[256,2048]{1,0:T(8,128)(2,1)S(1)}, bf16[256,2048]{1,0:T(8,128)(2,1)}, u32[]{:S(2)}) copy-start(bf16[256,2048]{1,0:T(8,128)(2,1)} %param.26) | copy-start | bytes 3145732
  6.6 98.1 %all-gather.3.cloned.1.call-start = ((), (), s32[]{:S(2)}) async-start(), calls=%async_computation.6 | async-start | bytes 5406720 | tf_op jit(solution)/shard_map/all_gather | solution.py:23
  104.7 3.1 copy-start.8
  104.7 3.1 copy-start.10
  107.8 3.7 copy-start.3
  126.8 11.0 %copy-start.9 = (bf16[256,256]{1,0:T(8,128)(2,1)S(1)}, bf16[256,256]{1,0:T(8,128)(2,1)}, u32[]{:S(2)}) copy-start(bf16[256,256]{1,0:T(8,128)(2,1)} %get-tuple-element.46) | copy-start | bytes 393220 | tf_op jit(solution)/shard_map/cond
  137.8 7.0 %copy-start.1 = (f32[2,256,8192]{1,2,0:T(8,128)S(1)}, f32[2,256,8192]{1,2,0:T(8,128)}, u32[]{:S(2)}) copy-start(f32[2,256,8192]{1,2,0:T(8,128)} %get-tuple-element.53) | copy-start | bytes 50331652 | tf_op jit(solution)/shard_map/cond
  156.0 5.8 %copy-start.7 = (s32[64,2]{0,1:T(2,128)S(1)}, s32[64,2]{0,1:T(2,128)}, u32[]{:S(2)}) copy-start(s32[64,2]{0,1:T(2,128)} %param.28) | copy-start | bytes 1540
  156.0 21.6 %copy-start.2 = (bf16[64,2048]{1,0:T(8,128)(2,1)S(1)}, bf16[64,2048]{1,0:T(8,128)(2,1)}, u32[]{:S(2)}) copy-start(bf16[64,2048]{1,0:T(8,128)(2,1)} %param.18) | copy-start | bytes 786436
  156.0 21.6 %copy-start.4 = (f32[2048]{0:T(1024)S(1)}, f32[2048]{0:T(1024)}, u32[]{:S(2)}) copy-start(f32[2048]{0:T(1024)} %param.27) | copy-start | bytes 24580
  156.0 21.8 %copy-start.5 = (f32[2048]{0:T(1024)S(1)}, f32[2048]{0:T(1024)}, u32[]{:S(2)}) copy-start(f32[2048]{0:T(1024)} %param.30) | copy-start | bytes 24580
  157.5 19.7 %all-to-all-start = ((bf16[4,64,2048]{2,1,0:T(8,128)(2,1)}), bf16[4,64,2048]{2,1,0:T(8,128)(2,1)S(1)}, u32[]{:S(2)}, u32[]{:S(2)}) async-start(bf16[4,64,2048]{2,1,0:T(8,128)(2,1)} %bitcast.8), calls=%async_computation | async-start | bytes 2097152 | tf_op jit(solution)/shard_map/all_to_all | solution.py:34
  161.7 111.1 %all-gather.5.cloned.1.call-start = ((), (), s32[]{:S(2)}) async-start(), calls=%async_computation.7 | async-start | bytes 3932160 | tf_op jit(solution)/shard_map/all_gather | solution.py:197
  339.3 59.3 %copy-start.6 = (f32[64,2]{0,1:T(2,128)S(1)}, f32[64,2]{0,1:T(2,128)}, u32[]{:S(2)}) copy-start(f32[64,2]{0,1:T(2,128)} %param.29) | copy-start | bytes 1540
Sparse Core Ops, SparseCore 0:
  9.3 95.3 all-gather.2
  234.6 38.2 all-gather.4
where the time goes:
time: 407 us
  blocking collectives  154 us (38%)
  waiting for transfers between devices  147 us (36%)
  matrix products  52 us (13%)
  other arithmetic  24.4 us (6%)
  between operations  13.7 us (3%)
  local copies, waits for them, and re-layouts  10.8 us (3%)
  starting transfers between devices  4.23 us (1%)
    all_to_all x4, blocking collectives, exchange_in_order(): result = lax.all_to_all(result, axes[k], k, k, tiled=True)  111 us
    all_gather x1, waiting for transfers between devices, side_by_side(): result = lax.all_gather(both, axis, axis=dim, tiled=True)  94.3 us
    all_to_all x1, blocking collectives, summed_on_arrival(): lax.all_to_all(split_up(array, dim, length), axis, 0, 0, tiled=True)  43 us
    all_gather x1, waiting for transfers between devices, body(): span_rows = lax.all_gather(received, 'tp', axis=0, tiled=True)  38.4 us
    all_to_all x1, waiting for transfers between devices, summed_on_arrival(): lax.all_to_all(split_up(array, dim, length), axis, 0, 0, tiled=True)  14.5 us
    dot_general x1, matrix products, body(): product = jnp.dot(chosen, w_down[0], preferred_element_type=jnp.float32)  12.2 us
    dot_general x1, matrix products, update(): jnp.einsum('thd,sd->hts', query_turned, key_turned, preferred_element_typ...  11 us
  transfers between devices with their start and end apart: 3, of which 3 were waited for; matrix products, arithmetic and copies ran while one was open for 1% of the time, Pallas kernels for 0%

commit v1 on v0

--- a/solution.py
+++ b/solution.py
@@ -1,19 +1,343 @@
+import functools
+
 import jax
 import jax.numpy as jnp
+import numpy as np
 from jax import lax
-from jax.sharding import Mesh
+from jax.experimental import pallas as pl
+from jax.experimental.pallas import tpu as pltpu
 from jax.sharding import PartitionSpec as P
+
+MESH = pl.DeviceIdType.MESH
+BF = jnp.bfloat16
+F32 = jnp.float32
+epsilon = 1e-06
+GROUPS = 4
+QUARTERS = 4
+
+
+def remote(src, dst, send_sem, recv_sem, device):
+    return pltpu.make_async_remote_copy(
+        src_ref=src, dst_ref=dst, send_sem=send_sem, recv_sem=recv_sem,
+        device_id=device, device_id_type=MESH,
+    )
+
+
+def rms_scale(inputs, gain_vector):
+    mean_square = jnp.mean(inputs * inputs, axis=-1, keepdims=True)
+    return inputs * lax.rsqrt(mean_square + epsilon) * gain_vector
+
+
+def dot(a, b, dims=((1,), (0,))):
+    return lax.dot_general(a, b, (dims, ((), ())), preferred_element_type=F32)
+
+
+def moe_kernel(
+    n_sp, n_tp, cap,
+    updated_ref, routes_ref, weight_ref, gain_ref, fold_ref, unfold_ref, wg_hbm, wu_hbm, wd_hbm,
+    out_ref,
+    wg, wu, wd, spots, send, recv, rows_in, hidden, partial, opposite, joined, arrived, back, returned,
+    w_sem, zs, zr, xs, xr, ys, yr, rs, rr,
+):
+    n_z = n_sp // 2
+    sp, tp = lax.axis_index("sp"), lax.axis_index("tp")
+    z, core = lax.div(sp, 2), lax.rem(sp, 2)
+    right, left = lax.rem(tp + 1, n_tp), lax.rem(tp + n_tp - 1, n_tp)
+    tok, width = updated_ref.shape
+    part = width // QUARTERS
+    half = width // 2
+    block = cap * QUARTERS
+    per = n_z // GROUPS
+    own_rows = per * 2 * cap
+
+    loads = [
+        pltpu.make_async_copy(src.at[0], dst, w_sem.at[i])
+        for i, (src, dst) in enumerate(((wg_hbm, wg), (wu_hbm, wu), (wd_hbm, wd)))
+    ]
+    for load in loads:
+        load.start()
+
+    barrier = pltpu.get_barrier_semaphore()
+
+    def greet(i, carry):
+        pl.semaphore_signal(barrier, inc=1, device_id={"sp": lax.rem(sp + i, n_sp)}, device_id_type=MESH)
+        return carry
+
+    lax.fori_loop(1, n_sp, greet, 0)
+    for i in range(1, n_tp):
+        pl.semaphore_signal(barrier, inc=1, device_id={"tp": lax.rem(tp + i, n_tp)}, device_id_type=MESH)
+
+    updated = updated_ref[...].astype(F32)
+    moe_in = rms_scale(updated, gain_ref[...]).astype(BF)
+    stacked = jnp.concatenate([moe_in[:, q * part:(q + 1) * part] for q in range(QUARTERS)], axis=0)
+
+    expert_ids = lax.broadcasted_iota(jnp.int32, (tok, n_sp), 1)
+    chosen = [routes_ref[:, k:k + 1] for k in range(2)]
+    hits = [(chosen[k] == expert_ids).astype(F32) for k in range(2)]
+    earlier = (
+        lax.broadcasted_iota(jnp.int32, (tok, tok), 1) < lax.broadcasted_iota(jnp.int32, (tok, tok), 0)
+    ).astype(F32).astype(BF)
+    order = dot(earlier, (hits[0] + hits[1]).astype(BF))
+    slots = lax.broadcasted_iota(jnp.int32, (tok, n_sp * block), 1)
+    for k in range(2):
+        place = jnp.sum(order * hits[k], axis=1, keepdims=True).astype(jnp.int32)
+        ahead = (lax.shift_right_logical(chosen[k], 1) - z + n_z) & (n_z - 1)
+        turn = jnp.where(ahead < n_z // 2, n_z - 1 - 2 * ahead, 2 * ahead - n_z)
+        first = (2 * turn + (chosen[k] & 1)) * block + place
+        for q in range(QUARTERS):
+            spots[k, q * tok:(q + 1) * tok, :] = (slots == first + q * cap).astype(F32).astype(BF)
+    sending = dot(spots[0] + spots[1], stacked, ((0,), (0,)))
+    for i in range(n_sp):
+        send[i // 2, i % 2] = sending[i * block:(i + 1) * block].astype(BF)
+
+    pl.semaphore_wait(barrier, n_sp - 1 + n_tp - 1)
+
+    def ahead_of(k):
+        return jnp.where(lax.rem(k, 2) == 1, lax.div(n_z - 1 - k, 2), lax.div(n_z + k, 2))
+
+    def dispatch_copy(k, to_core):
+        target = lax.rem(z + ahead_of(k), n_z) * 2 + to_core
+        return remote(send.at[k, to_core], recv.at[k, core], zs.at[k, to_core], zr.at[k, core], {"sp": target})
+
+    def dispatch_arrival(k, from_core):
+        return remote(send.at[k, from_core], recv.at[k, from_core], zs.at[k, from_core], zr.at[k, from_core], {"sp": sp})
+
+    def return_copy(k, to_core):
+        target = lax.rem(z - ahead_of(k) + n_z, n_z) * 2 + to_core
+        return remote(back.at[k, to_core], returned.at[k, core], rs.at[k, to_core], rr.at[k, core], {"sp": target})
+
+    def return_arrival(k, from_core):
+        return remote(back.at[k, from_core], returned.at[k, from_core], rs.at[k, from_core], rr.at[k, from_core], {"sp": sp})
+
+    last = n_z - 1
+
+    def start_dispatch(k, carry):
+        for to_core in range(2):
+            @pl.when(jnp.logical_or(k < last, core != to_core))
+            def _():
+                dispatch_copy(k, to_core).start()
+        return carry
+
+    lax.fori_loop(0, n_z, start_dispatch, 0)
+    recv[last, core] = send[last, core]
+
+    def to_right(src, dst, ss, rr_, i, j):
+        return remote(src, dst, ss.at[i, j], rr_.at[i, j], {"tp": right})
+
+    def to_left(src, dst, ss, rr_, i, j):
+        return remote(src, dst, ss.at[i, j], rr_.at[i, j], {"tp": left})
+
+    low, high = pl.ds(0, half), pl.ds(half, half)
+
+    def gather_copies(g):
+        return (
+            to_right(rows_in.at[g, 0], rows_in.at[g, 1], xs, xr, g, 0),
+            to_left(rows_in.at[g, 0], rows_in.at[g, 2], xs, xr, g, 1),
+            to_right(rows_in.at[g, 1, :, low], rows_in.at[g, 3, :, low], xs, xr, g, 2),
+            to_left(rows_in.at[g, 2, :, high], rows_in.at[g, 3, :, high], xs, xr, g, 3),
+        )
+
+    def reduce_copies(g):
+        return (
+            to_right(partial.at[g, 3, :, low], opposite.at[g, 0], ys, yr, g, 0),
+            to_left(partial.at[g, 3, :, high], opposite.at[g, 1], ys, yr, g, 1),
+            to_right(partial.at[g, 2, :, high], arrived.at[g, 0, :, high], ys, yr, g, 2),
+            to_left(partial.at[g, 1, :, low], arrived.at[g, 1, :, low], ys, yr, g, 3),
+            to_right(joined.at[g, 0], arrived.at[g, 0, :, low], ys, yr, g, 4),
+            to_left(joined.at[g, 1], arrived.at[g, 1, :, high], ys, yr, g, 5),
+        )
+
+    def collect(g):
+        for i in range(per):
+            for from_core in range(2):
+                k = g * per + i
+
+                @pl.when(jnp.logical_or(k < last, core != from_core))
+                def _():
+                    dispatch_arrival(k, from_core).wait_recv()
+        raw = recv[pl.ds(g * per, per)].reshape(per * 2 * block, part)
+        rows = dot(fold_ref[...], raw).astype(BF)
+        for q in range(QUARTERS):
+            rows_in[g, 0, :, q * part:(q + 1) * part] = rows[q * own_rows:(q + 1) * own_rows]
+        copies = gather_copies(g)
+        copies[0].start()
+        copies[1].start()
+
+    def pass_on(g):
+        copies = gather_copies(g)
+        copies[0].wait_recv()
+        copies[2].start()
+        copies[1].wait_recv()
+        copies[3].start()
+
+    def experts(g):
+        @pl.when(g == 0)
+        def _():
+            for load in loads:
+                load.wait()
+
+        copies = gather_copies(g)
+        copies[2].wait_recv()
+        copies[3].wait_recv()
+        rows = rows_in[g].reshape(n_tp * own_rows, width)
+        gate = dot(rows, wg[...])
+        up = dot(rows, wu[...])
+        hidden[...] = (gate / (1.0 + jnp.exp(-gate)) * up).astype(BF)
+        step = 512
+        for n in range(width // step):
+            down = dot(hidden[...], wd[:, n * step:(n + 1) * step]).astype(BF)
+            partial[g, :, :, n * step:(n + 1) * step] = down.reshape(n_tp, own_rows, step)
+        for copy in reduce_copies(g)[:4]:
+            copy.start()
+
+    def add_opposite(g):
+        copies = reduce_copies(g)
+        copies[0].wait_recv()
+        joined[g, 0] = (partial[g, 2, :, :half].astype(F32) + opposite[g, 0].astype(F32)).astype(BF)
+        copies[4].start()
+        copies[1].wait_recv()
+        joined[g, 1] = (partial[g, 1, :, half:].astype(F32) + opposite[g, 1].astype(F32)).astype(BF)
+        copies[5].start()
+
+    def give_back(g):
+        for copy in reduce_copies(g)[2:]:
+            copy.wait_recv()
+        total = (
+            partial[g, 0].astype(F32) + arrived[g, 0].astype(F32) + arrived[g, 1].astype(F32)
+        ).astype(BF)
+        stack = jnp.concatenate([total[:, q * part:(q + 1) * part] for q in range(QUARTERS)], axis=0)
+        blocks = dot(unfold_ref[...], stack)
+        for i in range(2 * per):
+            back[g * per + i // 2, i % 2] = blocks[i * block:(i + 1) * block].astype(BF)
+        for i in range(per):
+            for to_core in range(2):
+                k = g * per + i
+
+                @pl.when(jnp.logical_or(k < last, core != to_core))
+                def _():
+                    return_copy(k, to_core).start()
+
+    def step(g, carry):
+        @pl.when(g < GROUPS)
+        def _():
+            collect(g)
+
+        @pl.when(g > 0)
+        def _():
+            add_opposite(g - 1)
+
+        @pl.when(g < GROUPS)
+        def _():
+            pass_on(g)
+
+        @pl.when(g > 0)
+        def _():
+            give_back(g - 1)
+
+        @pl.when(g < GROUPS)
+        def _():
+            experts(g)
+
+        return carry
+
+    lax.fori_loop(0, GROUPS + 1, step, 0)
+    returned[last, core] = back[last, core]
+
+    def finish_turn(k, carry):
+        for other in range(2):
+            @pl.when(jnp.logical_or(k < last, core != other))
+            def _():
+                dispatch_copy(k, other).wait_send()
+                return_copy(k, other).wait_send()
+                return_arrival(k, other).wait_recv()
+        return carry
+
+    lax.fori_loop(0, n_z, finish_turn, 0)
+
+    def finish_group(g, carry):
+        for copy in gather_copies(g) + reduce_copies(g):
+            copy.wait_send()
+        return carry
+
+    lax.fori_loop(0, GROUPS, finish_group, 0)
+
+    outs = returned[...].reshape(n_sp * block, part)
+    first = dot(spots[0], outs)
+    second = dot(spots[1], outs)
+    for q in range(QUARTERS):
+        columns = pl.ds(q * part, part)
+        near = slice(q * tok, (q + 1) * tok)
+        out_ref[:, columns] = (
+            updated_ref[:, columns].astype(F32)
+            + first[near] * weight_ref[:, 0:1]
+            + second[near] * weight_ref[:, 1:2]
+        ).astype(BF)
+
+
+def fold_matrices(sources, cap):
+    rows = sources * cap * QUARTERS
+    fold = np.zeros((rows, rows), np.float32)
+    for q in range(QUARTERS):
+        for source in range(sources):
+            for slot in range(cap):
+                fold[(q * sources + source) * cap + slot, (source * QUARTERS + q) * cap + slot] = 1.0
+    return jnp.asarray(fold, BF), jnp.asarray(fold.T, BF)
+
+
+def moe(updated, routes, route_weight, moe_gain, w_gate, w_up, w_down):
+    n_sp, n_tp = lax.axis_size("sp"), lax.axis_size("tp")
+    tok, width = updated.shape
+    ff = w_gate.shape[2]
+    cap = max(2, 3 * tok // n_sp)
+    n_z = n_sp // 2
+    block, part, half = cap * QUARTERS, width // QUARTERS, width // 2
+    per = n_z // GROUPS
+    own = per * 2 * cap
+    fold, unfold = fold_matrices(per * 2, cap)
+    vmem = pl.BlockSpec(memory_space=pltpu.VMEM)
+    hbm = pl.BlockSpec(memory_space=pl.ANY)
+    dma = pltpu.SemaphoreType.DMA
+    return pl.pallas_call(
+        functools.partial(moe_kernel, n_sp, n_tp, cap),
+        out_shape=jax.ShapeDtypeStruct((tok, width), BF),
+        in_specs=[vmem] * 6 + [hbm] * 3,
+        out_specs=vmem,
+        scratch_shapes=[
+            pltpu.VMEM((width, ff), BF),
+            pltpu.VMEM((width, ff), BF),
+            pltpu.VMEM((ff, width), BF),
+            pltpu.VMEM((2, QUARTERS * tok, n_sp * block), BF),
+            pltpu.VMEM((n_z, 2, block, part), BF),
+            pltpu.VMEM((n_z, 2, block, part), BF),
+            pltpu.VMEM((GROUPS, n_tp, own, width), BF),
+            pltpu.VMEM((n_tp * own, ff), BF),
+            pltpu.VMEM((GROUPS, n_tp, own, width), BF),
+            pltpu.VMEM((GROUPS, 2, own, half), BF),
+            pltpu.VMEM((GROUPS, 2, own, half), BF),
+            pltpu.VMEM((GROUPS, 2, own, width), BF),
+            pltpu.VMEM((n_z, 2, block, part), BF),
+            pltpu.VMEM((n_z, 2, block, part), BF),
+            dma((3,)),
+            dma((n_z, 2)), dma((n_z, 2)),
+            dma((GROUPS, 4)), dma((GROUPS, 4)),
+            dma((GROUPS, 6)), dma((GROUPS, 6)),
+            dma((n_z, 2)), dma((n_z, 2)),
+        ],
+        compiler_params=pltpu.CompilerParams(
+            collective_id=1, has_side_effects=True, vmem_limit_bytes=60 * 1024 * 1024
+        ),
+    )(updated, routes, route_weight, moe_gain.reshape(1, -1), fold, unfold, w_gate, w_up, w_down)
+
 
 HEADS = 8
 NOPE = 128
 ROPE = 64
 VDIM = 128
-SP = ("sp_0", "sp_1")
-GRP_SP_TP = ("grp", "sp_0", "sp_1", "tp")
-GRP_SP = ("grp", "sp_0", "sp_1")
-
-
-epsilon = 1e-06
+SP = "sp"
+GRP_SP_TP = ("grp", "sp", "tp")
+GRP_SP = ("grp", "sp")
+
+
 rope_base = 10000.0
 
 
@@ -33,31 +357,6 @@
     length = lax.axis_size(axis)
     pieces = lax.all_to_all(split_up(array, dim, length), axis, 0, 0, tiled=True)
     return jnp.sum(pieces.astype(jnp.float32), axis=0)
-
-
-def in_order(pieces, dim):
-    dims = list(pieces.shape[1:])
-    dims[dim] *= pieces.shape[0]
-    return jnp.moveaxis(pieces, 0, dim).reshape(dims)
-
-
-def exchange_in_order(pieces, axes, order):
-    inside = pieces.shape[1:]
-    result = pieces.reshape(*(lax.axis_size(a) for a in axes), *inside)
-    for k in order:
-        result = lax.all_to_all(result, axes[k], k, k, tiled=True)
-    return result.reshape(-1, *inside)
-
-
-def two_step_exchange(array, groups, order, split_dim, concat_dim):
-    length = lax.axis_size(groups[0]) * lax.axis_size(groups[1])
-    pieces = split_up(array, split_dim, length)
-    return in_order(exchange_in_order(pieces, groups, order), concat_dim)
-
-
-def rms_scale(inputs, gain_vector):
-    mean_square = jnp.mean(inputs * inputs, axis=-1, keepdims=True)
-    return inputs * lax.rsqrt(mean_square + epsilon) * gain_vector
 
 
 def tables(positions, rot_width):
@@ -176,44 +475,10 @@
         product.astype(jnp.bfloat16).astype(jnp.float32).astype(jnp.bfloat16), "tp", 0
     )
     updated = (residual.astype(jnp.float32) + rms_scale(branch, post_gain)).astype(jnp.bfloat16)
-    moe_in = rms_scale(updated.astype(jnp.float32), moe_gain).astype(jnp.bfloat16)
-    token_count = routes.shape[0]
-    experts = lax.axis_size(SP)
-    capacity = max(2, 3 * token_count // experts)
-    onehot = (routes[:, :, None] == jnp.arange(experts, dtype=jnp.int32)[None, None, :]).astype(
-        jnp.int32
-    )
-    flat_hits = onehot.reshape(token_count * 2, experts)
-    order_in = jnp.cumsum(flat_hits, axis=0) - flat_hits
-    slot_ids = jnp.sum(
-        (order_in + jnp.arange(experts, dtype=jnp.int32)[None, :] * capacity) * flat_hits, axis=1
-    )
-    placing = slot_ids[:, None] == jnp.arange(experts * capacity, dtype=jnp.int32)[None, :]
-    placing = placing.astype(jnp.bfloat16).reshape(token_count, 2, experts * capacity)
-    sending = jnp.einsum("tks,td->sd", placing, moe_in, preferred_element_type=jnp.float32).astype(
-        jnp.bfloat16
-    )
-    received = two_step_exchange(sending, ("sp_0", "sp_1"), (1, 0), 0, 0)
-    span_rows = lax.all_gather(received, "tp", axis=0, tiled=True)
-    gate_pre = jnp.dot(span_rows, w_gate[0], preferred_element_type=jnp.float32)
-    up_proj = jnp.dot(span_rows, w_up[0], preferred_element_type=jnp.float32)
-    hidden_rows = (jax.nn.silu(gate_pre) * up_proj).astype(jnp.bfloat16)
-    chosen = hidden_rows
-    product = jnp.dot(chosen, w_down[0], preferred_element_type=jnp.float32)
-    expert_out = summed_on_arrival(
-        product.astype(jnp.bfloat16).astype(jnp.float32).astype(jnp.bfloat16), "tp", 0
-    ).astype(jnp.bfloat16)
-    returned = two_step_exchange(expert_out, ("sp_0", "sp_1"), (1, 0), 0, 0)
-    gathered_back = jnp.einsum("tks,sd->tkd", placing, returned, preferred_element_type=jnp.float32)
-    weighted = jnp.sum(gathered_back * route_weight[:, :, None], axis=1)
-    return (updated.astype(jnp.float32) + weighted).astype(jnp.bfloat16)
+    return moe(updated, routes, route_weight, moe_gain, w_gate, w_up, w_down)
 
 
 def solution(mesh):
-    torus = Mesh(
-        mesh.devices.reshape(mesh.shape["grp"], 16, 2, mesh.shape["tp"]),
-        ("grp", "sp_0", "sp_1", "tp"),
-    )
     placed = (
         P(GRP_SP_TP, None),
         P(GRP_SP, "tp"),
@@ -233,5 +498,5 @@
         P(SP, "tp", None),
     )
     return jax.shard_map(
-        body, mesh=torus, in_specs=placed, out_specs=P(GRP_SP_TP, None), check_vma=False
-    )
+        body, mesh=mesh, in_specs=placed, out_specs=P(GRP_SP_TP, None), check_vma=False
+    )

time: 407 us -> 300 us (0.74)
  blocking collectives: 154 us -> 0 us
  Pallas kernels: 0 us -> 111 us
  waiting for transfers between devices: 147 us -> 108 us
  matrix products: 52 us -> 31.1 us
    all_to_all x5 -> x0, blocking collectives: 154 us -> none  [the longest x4 111 us: exchange_in_order(): result = lax.all_to_all(result, axes[k], k, k, tiled=True)]
    pallas_call x0 -> x1, Pallas kernels: none -> 111 us  [moe(): pl.pallas_call(functools.partial(moe_kernel, n_sp, n_tp, cap), out_shape=...]
    all_gather x1 -> x0, waiting for transfers between devices: 38.4 us -> none  [body(): span_rows = lax.all_gather(received, 'tp', axis=0, tiled=True)]
    dot_general x4 -> x0, matrix products: 20.9 us -> none  [the longest x1 12.2 us: body(): product = jnp.dot(chosen, w_down[0], preferred_element_type=jnp.float32)]
  transfers between devices with their start and end apart: 3 -> 2, of which waited for: 3 -> 2; matrix products, arithmetic and copies ran while one was open for 1% -> 1% of each run, Pallas kernels for 0% -> 0%
where the time goes in v1:
time: 300 us; the launch traced here: 298 us
  Pallas kernels  111 us (37%)
  waiting for transfers between devices  108 us (36%)
  matrix products  31.1 us (10%)
  other arithmetic  21.1 us (7%)
  between operations  13.5 us (4%)
  local copies, waits for them, and re-layouts  8.37 us (3%)
  starting transfers between devices  4.23 us (1%)
    pallas_call x1, Pallas kernels, moe(): pl.pallas_call(functools.partial(moe_kernel, n_sp, n_tp, cap), out_shape=...  111 us
    all_gather x1, waiting for transfers between devices, side_by_side(): result = lax.all_gather(both, axis, axis=dim, tiled=True)  94.3 us
    all_to_all x1, waiting for transfers between devices, summed_on_arrival(): lax.all_to_all(split_up(array, dim, length), axis, 0, 0, tiled=True)  14.1 us
    dot_general x1, matrix products, update(): jnp.einsum('thd,sd->hts', query_turned, key_turned, preferred_element_typ...  11 us
    dot_general x1, matrix products, update(): jnp.einsum('thd,shd->hts', query_plain, key_heads, preferred_element_type...  8.09 us
    reduce_sum x1, other arithmetic, update(): row_sum = jnp.sum(weights, axis=-1)  7.96 us
  transfers between devices with their start and end apart: 2, of which 2 were waited for; matrix products, arithmetic and copies ran while one was open for 1% of the time, Pallas kernels for 0%

profile of v1, /device:TPU:40, one launch (start us, length us, event | category | flops | bytes accessed | tf_op | source)
XLA Modules:
  0.0 297.9 jit_solution(13071725588879375481)
XLA Ops:
  6.5 0.0 copy-start
  6.6 0.0 all-gather.2.cloned.1.call-start
  6.6 1.1 copy.35
  7.6 1.4 pad_maximum_fusion
  9.1 0.1 all-gather.2.cloned.1.call-update
  9.2 0.9 copy.36
  10.1 0.2 multiply_cosine_fusion.1
  10.4 94.3 %all-gather.2.cloned.1.call-done = bf16[8192,320]{0,1:T(8,128)(2,1)} async-done(((bf16[256,320]{0,1:T(8,128)(2,1)}), bf16[8192,320]{0,1:T(8,128)(2,1)}) %all-gather.2.cloned.1.call-update) | async-done | bytes 5242896 | tf_op jit(solution)/shard_map/all_gather | solution.py:347
  104.7 0.0 copy-start.5
  104.7 0.0 copy-start.6
  104.7 51.2 %conditional.1 = (f32[2,256]{1,0:T(2,128)S(1)}, f32[2,256,128]{1,2,0:T(8,128)S(1)}) conditional(s32[]{:T(128)} %convert_element_type.73, () %tuple.13, (s32[]{:T(128)}, s32[256]{0:T(256)S(1)}, bf16[8192,320]{0,1:T(8,128)(2,1)}, f32[256]{0:T(256)}, bf16[256,256]{1,0:T(8,128)(2,1)}, /*index=5*/bf16[256,256]{1,0:T(8,128)(2,1)}, ...), branch_computations={%region_0.0_spmd, %region_1.5_spmd} | conditional | flops 4899749888 | bytes 193910160 | solution.py:469
  104.7 3.1 %fusion.4 = f32[8192]{0:T(1024)S(1)} fusion(bf16[8192,320]{0,1:T(8,128)(2,1)} %get-tuple-element.29), kind=kLoop, calls=%fused_computation.10 | loop fusion | flops 6283264 | bytes 4227072 | tf_op jit(solution)/shard_map/cond/branch_1_fun/reduce_sum | solution.py:27
  107.8 0.0 copy-start.3
  107.8 3.7 %convolution_convert_fusion.1 = bf16[8192,256]{0,1:T(8,128)(2,1)S(1)} fusion(bf16[256,256]{1,0:T(8,128)(2,1)} %get-tuple-element.44, f32[256]{0:T(256)} %get-tuple-element.43, f32[8192]{0:T(1024)S(1)} %add_rsqrt_fusion, bf16[8192,320]{0,1:T(8,128)(2,1)} %get-tuple-element.29), kind=kOutput, calls=%fused_computation.9 | convolution fusion | flops 1084227584 | bytes 8553472 | tf_op jit(solution)/shard_map/cond/branch_1_fun/dot_general | solution.py:383
  111.5 0.0 copy-done.3
  111.5 8.1 %fusion.22 = f32[2,8192,256]{2,1,0:T(8,128)} fusion(bf16[8192,2,128]{0,2,1:T(8,128)(2,1)S(1)} %bitcast.35, bf16[256,256]{1,0:T(8,128)(2,1)S(1)} %copy-done.3), kind=kOutput, calls=%fused_computation.30 | convolution fusion | flops 1073741824 | bytes 21102592 | tf_op jit(solution)/shard_map/cond/branch_1_fun/thd,shd->hts/dot_general | solution.py:430
  119.6 1.4 slice_convert_fusion
  121.0 4.4 %fusion.15 = (bf16[8192,32]{0,1:T(8,128)(2,1)S(1)}, bf16[8192,32]{0,1:T(8,128)(2,1)S(1)}) fusion(f32[8192,64]{0,1:T(8,128)S(1)} %slice_convert_fusion, f32[32]{0:T(128)S(1)} %negate_power_fusion, f32[8192]{0:T(1024)S(1)} %iota_convert_fusion), kind=kLoop, calls=%fused_computation.23 | loop fusion | flops 2359296 | bytes 3178624 | tf_op jit(solution)/shard_map/convert
  125.4 1.4 iota_compare_fusion
  126.8 0.0 copy-start.7
  126.8 0.0 copy-start.8
  126.8 11.0 %fusion.26 = (f32[2,256]{1,0:T(2,128)S(1)}, f32[2,256,8192]{1,2,0:T(8,128)}) fusion(bf16[256,2,64]{0,2,1:T(8,128)(2,1)S(1)} %get-tuple-element.33, bf16[8192,32]{0,1:T(8,128)(2,1)S(1)} %get-tuple-element.49, bf16[8192,32]{0,1:T(8,128)(2,1)S(1)} %get-tuple-element.48, f32[2,8192,256]{2,1,0:T(8,128)} %fusion.22, pred[256,8192]{0,1:T(8,128)(4,1)S(1)} %iota_compare_fusion), kind=kOutput, calls=%fused_computation.53 | convolution fusion | flops 555744768 | bytes 36767744 | tf_op jit(solution)/shard_map/cond/branch_1_fun/thd,sd->hts/dot_general | solution.py:435
  137.8 0.0 copy-done.7
  137.8 0.0 copy-done.8
  137.8 0.0 copy-start.1
  137.8 3.8 %convolution_convert_fusion = bf16[8192,256]{0,1:T(8,128)(2,1)S(1)} fusion(bf16[256,256]{1,0:T(8,128)(2,1)S(1)} %copy-done.7, f32[256]{0:T(256)S(1)} %copy-done.8, f32[8192]{0:T(1024)S(1)} %add_rsqrt_fusion, bf16[8192,320]{0,1:T(8,128)(2,1)} %get-tuple-element.29), kind=kOutput, calls=%fused_computation.8 | convolution fusion | flops 1084227584 | bytes 8553472 | tf_op jit(solution)/shard_map/cond/branch_1_fun/dot_general | solution.py:384
  141.6 3.2 %copy-done.1 = f32[2,256,8192]{1,2,0:T(8,128)S(1)} copy-done((f32[2,256,8192]{1,2,0:T(8,128)S(1)}, f32[2,256,8192]{1,2,0:T(8,128)}, u32[]{:S(2)}) %copy-start.1) | copy-done | bytes 16777240 | tf_op jit(solution)/shard_map/cond
  144.8 3.1 %fusion.7 = f32[2,256,128]{1,2,0:T(8,128)S(1)} fusion(bf16[8192,2,128]{0,2,1:T(8,128)(2,1)S(1)} %bitcast.36, f32[2,256,8192]{1,2,0:T(8,128)S(1)} %copy-done.1, f32[2,256]{1,0:T(2,128)S(1)} %broadcast_maximum_fusion), kind=kOutput, calls=%fused_computation.13 | convolution fusion | flops 1082130432 | bytes 21235712 | tf_op jit(solution)/shard_map/cond | solution.py:469
  148.0 8.0 %fusion.3 = f32[2,256]{1,0:T(2,128)S(1)} fusion(f32[2,256,8192]{1,2,0:T(8,128)} %get-tuple-element.51, f32[2,256]{1,0:T(2,128)S(1)} %broadcast_maximum_fusion), kind=kLoop, calls=%fused_computation.5 | loop fusion | flops 8388096 | bytes 16781312 | tf_op jit(solution)/shard_map/cond/branch_1_fun/reduce_sum | solution.py:444
  155.9 0.0 copy-start.2
  155.9 0.0 copy-start.4
  156.0 0.0 copy-done
  156.0 1.4 convolution_convert_fusion.2
  157.4 4.2 %all-to-all-start = ((bf16[4,64,2048]{2,1,0:T(8,128)(2,1)}), bf16[4,64,2048]{2,1,0:T(8,128)(2,1)S(1)}, u32[]{:S(2)}, u32[]{:S(2)}) async-start(bf16[4,64,2048]{2,1,0:T(8,128)(2,1)} %bitcast.8), calls=%async_computation | async-start | bytes 2097152 | tf_op jit(solution)/shard_map/all_to_all | solution.py:358
  161.7 0.0 copy-done.5
  161.7 0.7 copy.38.routes_ref
  162.4 0.0 copy-done.6
  162.4 0.7 copy.39.weight_ref
  163.1 14.1 %all-to-all-done = bf16[4,64,2048]{2,1,0:T(8,128)(2,1)S(1)} async-done(((bf16[4,64,2048]{2,1,0:T(8,128)(2,1)}), bf16[4,64,2048]{2,1,0:T(8,128)(2,1)S(1)}, u32[]{:S(2)}, u32[]{:S(2)}) %all-to-all-start) | async-done | bytes 1048608 | tf_op jit(solution)/shard_map/all_to_all | solution.py:358
  177.2 0.2 convert_reduce_fusion
  177.3 0.1 multiply_reduce_fusion
  177.5 0.0 copy-done.2
  177.5 0.0 copy-done.4
  177.5 0.9 add_convert_fusion.updated_ref
  178.3 111.0 %shard_map.176 = bf16[64,2048]{1,0:T(8,128)(2,1)} custom-call(bf16[64,2048]{1,0:T(8,128)(2,1)} %add_convert_fusion.updated_ref, s32[64,2]{1,0:T(8,128)} %copy.38.routes_ref, f32[64,2]{1,0:T(8,128)} %copy.39.weight_ref, f32[1,2048]{1,0:T(1,128)} %bitcast.39, bf16[192,192]{1,0:T(8,128)(2,1)} %constant.58.clone.fold_ref, ...), custom_call_target="tpu_custom_call" | custom-call | tf_op jit(solution)/shard_map/pallas_call | solution.py:300
  289.4 1.7 copy.55
  (12 shorter events, 0.1 us)
Async XLA Ops:
  6.5 149.4 %copy-start = (bf16[256,2048]{1,0:T(8,128)(2,1)S(1)}, bf16[256,2048]{1,0:T(8,128)(2,1)}, u32[]{:S(2)}) copy-start(bf16[256,2048]{1,0:T(8,128)(2,1)} %param.28) | copy-start | bytes 3145732
  6.6 98.1 %all-gather.2.cloned.1.call-start = ((), (), s32[]{:S(2)}) async-start(), calls=%async_computation.1 | async-start | bytes 5406720 | tf_op jit(solution)/shard_map/all_gather | solution.py:347
  104.7 57.0 %copy-start.5 = (s32[64,2]{0,1:T(2,128)S(1)}, s32[64,2]{0,1:T(2,128)}, u32[]{:S(2)}) copy-start(s32[64,2]{0,1:T(2,128)} %param.30) | copy-start | bytes 1540
  104.7 57.7 %copy-start.6 = (f32[64,2]{0,1:T(2,128)S(1)}, f32[64,2]{0,1:T(2,128)}, u32[]{:S(2)}) copy-start(f32[64,2]{0,1:T(2,128)} %param.31) | copy-start | bytes 1540
  107.8 3.7 %copy-start.3 = (bf16[256,256]{1,0:T(8,128)(2,1)S(1)}, bf16[256,256]{1,0:T(8,128)(2,1)}, u32[]{:S(2)}) copy-start(bf16[256,256]{1,0:T(8,128)(2,1)} %get-tuple-element.45) | copy-start | bytes 393220 | tf_op jit(solution)/shard_map/cond
  126.8 11.0 %copy-start.7 = (bf16[256,256]{1,0:T(8,128)(2,1)S(1)}, bf16[256,256]{1,0:T(8,128)(2,1)}, u32[]{:S(2)}) copy-start(bf16[256,256]{1,0:T(8,128)(2,1)} %get-tuple-element.46) | copy-start | bytes 393220 | tf_op jit(solution)/shard_map/cond
  126.8 11.0 %copy-start.8 = (f32[256]{0:T(256)S(1)}, f32[256]{0:T(256)}, u32[]{:S(2)}) copy-start(f32[256]{0:T(256)} %get-tuple-element.43) | copy-start | bytes 3076 | tf_op jit(solution)/shard_map/cond
  137.8 7.0 %copy-start.1 = (f32[2,256,8192]{1,2,0:T(8,128)S(1)}, f32[2,256,8192]{1,2,0:T(8,128)}, u32[]{:S(2)}) copy-start(f32[2,256,8192]{1,2,0:T(8,128)} %get-tuple-element.51) | copy-start | bytes 50331652 | tf_op jit(solution)/shard_map/cond
  155.9 21.5 %copy-start.2 = (bf16[64,2048]{1,0:T(8,128)(2,1)S(1)}, bf16[64,2048]{1,0:T(8,128)(2,1)}, u32[]{:S(2)}) copy-start(bf16[64,2048]{1,0:T(8,128)(2,1)} %param.20) | copy-start | bytes 786436
  155.9 21.5 %copy-start.4 = (f32[2048]{0:T(1024)S(1)}, f32[2048]{0:T(1024)}, u32[]{:S(2)}) copy-start(f32[2048]{0:T(1024)} %param.29) | copy-start | bytes 24580
  157.4 19.7 %all-to-all-start = ((bf16[4,64,2048]{2,1,0:T(8,128)(2,1)}), bf16[4,64,2048]{2,1,0:T(8,128)(2,1)S(1)}, u32[]{:S(2)}, u32[]{:S(2)}) async-start(bf16[4,64,2048]{2,1,0:T(8,128)(2,1)} %bitcast.8), calls=%async_computation | async-start | bytes 2097152 | tf_op jit(solution)/shard_map/all_to_all | solution.py:358
Sparse Core Ops, SparseCore 0:
  9.3 95.3 all-gather.1

commit v2 on v1

--- a/solution.py
+++ b/solution.py
@@ -12,6 +12,10 @@
 BF = jnp.bfloat16
 F32 = jnp.float32
 epsilon = 1e-06
+rope_base = 10000.0
+SP = "sp"
+GRP_SP_TP = ("grp", "sp", "tp")
+GRP_SP = ("grp", "sp")
 GROUPS = 4
 QUARTERS = 4
 
@@ -329,65 +333,300 @@
     )(updated, routes, route_weight, moe_gain.reshape(1, -1), fold, unfold, w_gate, w_up, w_down)
 
 
-HEADS = 8
-NOPE = 128
-ROPE = 64
-VDIM = 128
-SP = "sp"
-GRP_SP_TP = ("grp", "sp", "tp")
-GRP_SP = ("grp", "sp")
-
-
-rope_base = 10000.0
-
-
-def side_by_side(arrays, axis, dim, along):
-    widths = [a.shape[along] for a in arrays]
-    both = jnp.concatenate(arrays, axis=along)
-    result = lax.all_gather(both, axis, axis=dim, tiled=True)
-    return tuple(jnp.split(result, [sum(widths[:k]) for k in range(1, len(widths))], axis=along))
-
-
-def split_up(array, dim, length):
-    before, after = (array.shape[:dim], array.shape[dim + 1 :])
-    return jnp.moveaxis(array.reshape(*before, length, -1, *after), dim, 0)
-
-
-def summed_on_arrival(array, axis, dim):
-    length = lax.axis_size(axis)
-    pieces = lax.all_to_all(split_up(array, dim, length), axis, 0, 0, tiled=True)
-    return jnp.sum(pieces.astype(jnp.float32), axis=0)
+def attention_kernel(
+    n_sp, n_tp, heads,
+    residual_ref, nope_ref, rope_ref, latent_ref, rope_key_ref, latent_gain_ref, cosine_ref, sine_ref,
+    w_key_ref, w_value_ref, w_out_ref, post_gain_ref,
+    updated_ref,
+    kv, q_send, q_recv, queries, top, total, running, values, outs,
+    ring_s, ring_r, side_s, side_r, q_s, q_r, w_s, w_r, p_s, p_r,
+):
+    n_z = n_sp // 2
+    sp, tp = lax.axis_index("sp"), lax.axis_index("tp")
+    z, core = lax.div(sp, 2), lax.rem(sp, 2)
+    right, left = lax.rem(tp + 1, n_tp), lax.rem(tp + n_tp - 1, n_tp)
+    rows, rank = latent_ref.shape
+    rot = rope_key_ref.shape[1]
+    nope = w_key_ref.shape[1] // heads
+    tok, width = residual_ref.shape
+    packs = rank // rot
+    span = rows // packs
+    block = rows + span
+    partner = {"sp": z * 2 + 1 - core}
+    up_chip = {"sp": lax.rem(z + 1, n_z) * 2 + core}
+    down_chip = {"sp": lax.rem(z + n_z - 1, n_z) * 2 + core}
+
+    barrier = pltpu.get_barrier_semaphore()
+    for device in (partner, up_chip, down_chip):
+        pl.semaphore_signal(barrier, inc=1, device_id=device, device_id_type=MESH)
+    for i in range(1, n_tp):
+        pl.semaphore_signal(barrier, inc=1, device_id={"tp": lax.rem(tp + i, n_tp)}, device_id_type=MESH)
+
+    def rotate(values, cosine, sine):
+        half = rot // 2
+        lane = lax.broadcasted_iota(jnp.int32, values.shape, 1)
+        wide = values.shape[1]
+        other = jnp.where(
+            (lane & half) == 0, pltpu.roll(values, wide - half, 1), pltpu.roll(values, half, 1)
+        )
+        return (values * cosine + other * sine).astype(BF)
+
+    normed = rms_scale(latent_ref[...].astype(F32), latent_gain_ref[...]).astype(BF)
+    kv[z, core, :rows] = normed
+    key_pair = jnp.concatenate([rope_key_ref[...]] * 2, axis=1).astype(F32)
+    key_turned = rotate(key_pair, cosine_ref[...], sine_ref[...])[:, :rot]
+    kv[z, core, rows:] = jnp.concatenate(
+        [key_turned[i * span:(i + 1) * span] for i in range(packs)], axis=1
+    )
+
+    pl.semaphore_wait(barrier, 2 + 1 + n_tp - 1)
+
+    cut = block // 2
+
+    def ring_copy(way, s, h):
+        chip = lax.rem(z - s + n_z, n_z) if way == 0 else lax.rem(z + s, n_z)
+        place = kv.at[chip, core, pl.ds(h * cut, cut)]
+        return remote(place, place, ring_s.at[way, s, h], ring_r.at[way, s, h], up_chip if way == 0 else down_chip)
+
+    def source_chip(way, s):
+        return lax.rem(z - 1 - s + n_z, n_z) if way == 0 else lax.rem(z + 1 + s, n_z)
+
+    def side_copy(way, s):
+        place = kv.at[source_chip(way, s), core]
+        return remote(place, place, side_s.at[way, s], side_r.at[way, s], partner)
+
+    far = n_z // 2
+    reach = (far, far - 1)
+    for h in range(2):
+        for way in range(2):
+            ring_copy(way, 0, h).start()
+    own = kv.at[z, core]
+    own_side = remote(own, own, side_s.at[1, far - 1], side_r.at[1, far - 1], partner)
+    own_side.start()
+
+    turned = rotate(rope_ref[...].astype(F32), cosine_ref[...], sine_ref[...])
+    for h in range(heads):
+        columns = slice(h * nope, (h + 1) * nope)
+        folded = dot(nope_ref[:, columns], w_key_ref[:, columns], ((1,), (1,))).astype(BF)
+        for i in range(n_tp):
+            q_send[i, :, h * rank:(h + 1) * rank] = folded[i * tok:(i + 1) * tok]
+    for i in range(n_tp):
+        q_send[i, :, heads * rank:] = turned[i * tok:(i + 1) * tok]
+
+    def q_copy(i):
+        to = lax.rem(tp + i, n_tp)
+        return remote(q_send.at[to], q_recv.at[i - 1], q_s.at[i - 1], q_r.at[i - 1], {"tp": to})
+
+    for i in (2, 1, 3):
+        q_copy(i).start()
+
+    shares = ((w_value_ref, values), (w_out_ref, outs))
+
+    def share_copies(a):
+        own_ref, whole = shares[a]
+        deep, wide = own_ref.shape
+        mine = pl.ds(core * (deep // 2), deep // 2)
+        low, high = pl.ds(0, wide // 2), pl.ds(wide // 2, wide // 2)
+        across = (
+            remote(own_ref.at[mine], whole.at[0, mine], w_s.at[a, 0], w_r.at[a, 0], {"tp": right}),
+            remote(own_ref.at[mine], whole.at[1, mine], w_s.at[a, 1], w_r.at[a, 1], {"tp": left}),
+            remote(whole.at[0, mine, low], whole.at[2, mine, low], w_s.at[a, 2], w_r.at[a, 2], {"tp": right}),
+            remote(whole.at[1, mine, high], whole.at[2, mine, high], w_s.at[a, 3], w_r.at[a, 3], {"tp": left}),
+        )
+        beside = tuple(
+            remote(whole.at[i, mine], whole.at[i, mine], p_s.at[a, i], p_r.at[a, i], partner) for i in range(3)
+        )
+        return across, beside
+
+    for a in range(2):
+        across, _ = share_copies(a)
+        across[0].start()
+        across[1].start()
+
+    def place_query(slot, sent):
+        for h in range(heads):
+            at = (slot * heads + h) * tok
+            queries[at:at + tok, :rank] = sent[:, h * rank:(h + 1) * rank]
+            queries[at:at + tok, rank:] = sent[:, heads * rank + h * rot:heads * rank + (h + 1) * rot]
+
+    place_query(0, q_send[tp])
+    top[...] = jnp.full(top.shape, -1e30, F32)
+    total[...] = jnp.zeros(total.shape, F32)
+    running[...] = jnp.zeros(running.shape, F32)
+    for i in (1, 3, 2):
+        q_copy(i).wait_recv()
+        place_query(i, q_recv[i - 1])
+
+    scale = (nope + rot) ** (-0.5) * 1.4426950408889634
+    lanes = total.shape[1]
+
+    def update(chip, masked):
+        latents = kv[chip, :, :rows].reshape(2 * rows, rank)
+        packed = kv[chip, :, rows:]
+        keys_turned = jnp.concatenate(
+            [packed[c, :, i * rot:(i + 1) * rot] for c in range(2) for i in range(packs)], axis=0
+        )
+        keys = jnp.concatenate([latents, keys_turned], axis=1)
+        scores = dot(queries[...], keys, ((1,), (1,))) * scale
+        if masked:
+            key_at = lax.broadcasted_iota(jnp.int32, scores.shape, 1)
+            row_at = (lax.broadcasted_iota(jnp.int32, scores.shape, 0) & (tok - 1)) + core * rows + tp * tok
+            scores = jnp.where(key_at <= row_at, scores, -1e30)
+        old = top[...]
+        new = jnp.maximum(old, jnp.max(scores, axis=1, keepdims=True))
+        shrink = jnp.exp2(old - new)
+        expo = jnp.exp2(scores - new)
+        added = expo[:, :lanes]
+        for i in range(1, 2 * rows // lanes):
+            added = added + expo[:, i * lanes:(i + 1) * lanes]
+        total[...] = total[...] * shrink + added
+        running[...] = running[...] * shrink + dot(expo.astype(BF), latents)
+        top[...] = new
+
+    own_side.wait_recv()
+    update(z, True)
+
+    def pass_half(s, h):
+        for way in range(2):
+            @pl.when(s < reach[way])
+            def _():
+                ring_copy(way, s, h).wait_recv()
+
+            @pl.when(s + 1 < reach[way])
+            def _():
+                ring_copy(way, s + 1, h).start()
+
+    def visit(way, s):
+        @pl.when(jnp.logical_and(s >= 0, s < reach[way]))
+        def _():
+            side_copy(way, s).wait_recv()
+
+            @pl.when(source_chip(way, s) < z)
+            def _():
+                update(source_chip(way, s), False)
+
+    def ring_step(s, carry):
+        pass_half(s, 0)
+        visit(0, s - 1)
+        pass_half(s, 1)
+        for way in range(2):
+            @pl.when(s < reach[way])
+            def _():
+                side_copy(way, s).start()
+        visit(1, s - 1)
+
+        @pl.when(s == far - 3)
+        def _():
+            for a in range(2):
+                across, beside = share_copies(a)
+                across[0].wait_recv()
+                across[2].start()
+                beside[0].start()
+                across[1].wait_recv()
+                across[3].start()
+                beside[1].start()
+
+        return carry
+
+    lax.fori_loop(0, far + 1, ring_step, 0)
+
+    for a in range(2):
+        across, beside = share_copies(a)
+        across[2].wait_recv()
+        across[3].wait_recv()
+        beside[2].start()
+
+    row_sum = jnp.sum(total[...], axis=1, keepdims=True)
+    mixed_latent = (running[...] / row_sum).astype(BF)
+    for a in range(2):
+        _, beside = share_copies(a)
+        for copy in beside:
+            copy.wait_recv()
+
+    branch = jnp.zeros((tok, width), F32)
+    for slot, kept in enumerate((None, 0, 2, 1)):
+        w_value = w_value_ref[...] if kept is None else values[kept]
+        w_out = w_out_ref[...] if kept is None else outs[kept]
+        attended = []
+        for h in range(heads):
+            at = (slot * heads + h) * tok
+            attended.append(dot(mixed_latent[at:at + tok], w_value[:, h * nope:(h + 1) * nope]).astype(BF))
+        branch = branch + dot(jnp.concatenate(attended, axis=1), w_out).astype(BF).astype(F32)
+    updated_ref[...] = (
+        residual_ref[...].astype(F32) + rms_scale(branch, post_gain_ref[...])
+    ).astype(BF)
+
+    def drain(s, carry):
+        for way in range(2):
+            @pl.when(s < reach[way])
+            def _():
+                for h in range(2):
+                    ring_copy(way, s, h).wait_send()
+                side_copy(way, s).wait_send()
+        return carry
+
+    lax.fori_loop(0, far, drain, 0)
+    own_side.wait_send()
+    for i in range(1, n_tp):
+        q_copy(i).wait_send()
+    for a in range(2):
+        across, beside = share_copies(a)
+        for copy in across + beside:
+            copy.wait_send()
+
+
+def attention(
+    residual, query_nope, query_rope, kv_latent, rope_key, latent_gain, w_key, w_value, w_out, post_gain
+):
+    n_sp, n_tp = lax.axis_size("sp"), lax.axis_size("tp")
+    tok, width = residual.shape
+    rows, rank = kv_latent.shape
+    rot = rope_key.shape[1]
+    heads = query_rope.shape[1] // rot
+    n_z = n_sp // 2
+    far = n_z // 2
+    positions = lax.axis_index("sp") * rows + jnp.arange(rows, dtype=jnp.int32)
+    cosine, sine = tables(positions, rot)
+    cosine = jnp.concatenate([cosine] * (2 * heads), axis=1)
+    sine = jnp.concatenate([-sine, sine] * heads, axis=1)
+    block = rows + rot * rows // rank
+    span = heads * rank + heads * rot
+    vmem = pl.BlockSpec(memory_space=pltpu.VMEM)
+    dma = pltpu.SemaphoreType.DMA
+    return pl.pallas_call(
+        functools.partial(attention_kernel, n_sp, n_tp, heads),
+        out_shape=jax.ShapeDtypeStruct((tok, width), BF),
+        in_specs=[vmem] * 12,
+        out_specs=vmem,
+        scratch_shapes=[
+            pltpu.VMEM((n_z, 2, block, rank), BF),
+            pltpu.VMEM((n_tp, tok, span), BF),
+            pltpu.VMEM((n_tp - 1, tok, span), BF),
+            pltpu.VMEM((n_tp * heads * tok, rank + rot), BF),
+            pltpu.VMEM((n_tp * heads * tok, 1), F32),
+            pltpu.VMEM((n_tp * heads * tok, 128), F32),
+            pltpu.VMEM((n_tp * heads * tok, rank), F32),
+            pltpu.VMEM((n_tp - 1,) + w_value.shape, BF),
+            pltpu.VMEM((n_tp - 1,) + w_out.shape, BF),
+            dma((2, far, 2)), dma((2, far, 2)),
+            dma((2, far)), dma((2, far)),
+            dma((n_tp - 1,)), dma((n_tp - 1,)),
+            dma((2, 4)), dma((2, 4)),
+            dma((2, 3)), dma((2, 3)),
+        ],
+        compiler_params=pltpu.CompilerParams(
+            collective_id=0, has_side_effects=True, vmem_limit_bytes=60 * 1024 * 1024
+        ),
+    )(
+        residual, query_nope, query_rope, kv_latent, rope_key, latent_gain.reshape(1, -1), cosine, sine,
+        w_key, w_value, w_out, post_gain.reshape(1, -1),
+    )
 
 
 def tables(positions, rot_width):
     frequency = 1.0 / rope_base ** (jnp.arange(0, rot_width, 2, dtype=jnp.float32) / rot_width)
     angles = positions.astype(jnp.float32)[:, None] * frequency[None, :]
     return (jnp.cos(angles), jnp.sin(angles))
-
-
-def rotate(inputs, cosine_table, sine_table):
-    half_width = inputs.shape[-1] // 2
-    first_half = inputs[..., :half_width]
-    second_half = inputs[..., half_width:]
-    return jnp.concatenate(
-        [
-            first_half * cosine_table - second_half * sine_table,
-            second_half * cosine_table + first_half * sine_table,
-        ],
-        axis=-1,
-    )
-
-
-def expand(latent_rows, rope_rows, latent_gain, w_key, w_value):
-    normed = rms_scale(latent_rows.astype(jnp.float32), latent_gain).astype(jnp.bfloat16)
-    key_plain = jnp.dot(normed, w_key, preferred_element_type=jnp.float32).astype(jnp.bfloat16)
-    value_plain = jnp.dot(normed, w_value, preferred_element_type=jnp.float32).astype(jnp.bfloat16)
-    key_positions = jnp.arange(latent_rows.shape[0], dtype=jnp.int32)
-    cosine_table, sine_table = tables(key_positions, rope_rows.shape[1])
-    key_turned = rotate(rope_rows.astype(jnp.float32), cosine_table, sine_table).astype(
-        jnp.bfloat16
-    )
-    return (key_plain, value_plain, key_turned)
 
 
 def body(
@@ -408,73 +647,9 @@
     w_up,
     w_down,
 ):
-    tok_rows = query_nope.shape[0]
-    heads_here = HEADS // lax.axis_size("tp")
-    first_row = lax.axis_index(SP) * tok_rows
-    last_row = first_row + tok_rows - 1
-    positions = first_row + jnp.arange(tok_rows, dtype=jnp.int32)
-    cosine_table, sine_table = tables(positions, ROPE)
-    query_plain = query_nope.reshape(tok_rows, heads_here, NOPE)
-    query_turned = rotate(
-        query_rope.reshape(tok_rows, heads_here, ROPE).astype(jnp.float32),
-        cosine_table[:, None, :],
-        sine_table[:, None, :],
-    ).astype(jnp.bfloat16)
-    score_scale = (NOPE + ROPE) ** (-0.5)
-
-    def update(state_now, key_plain, value_plain, key_turned):
-        row_max, row_sum, running = state_now
-        key_count = key_plain.shape[0]
-        key_heads = key_plain.reshape(key_count, heads_here, NOPE)
-        value_heads = value_plain.reshape(key_count, heads_here, VDIM)
-        scores = jnp.einsum(
-            "thd,shd->hts", query_plain, key_heads, preferred_element_type=jnp.float32
-        )
-        scores = (
-            scores
-            + jnp.einsum(
-                "thd,sd->hts", query_turned, key_turned, preferred_element_type=jnp.float32
-            )
-        ) * score_scale
-        key_positions = jnp.arange(key_count, dtype=jnp.int32)
-        allowed = key_positions[None, :] <= positions[:, None]
-        scores = jnp.where(allowed[None], scores, -1e30)
-        new_max = jnp.maximum(row_max, jnp.max(scores, axis=-1))
-        weights = jnp.exp(scores - new_max[..., None])
-        row_sum = jnp.sum(weights, axis=-1)
-        running = jnp.einsum(
-            "hts,shd->htd",
-            weights.astype(jnp.bfloat16),
-            value_heads,
-            preferred_element_type=jnp.float32,
-        )
-        return (new_max, row_sum, running)
-
-    start_state = (
-        jnp.full((heads_here, tok_rows), -1e30, jnp.float32),
-        jnp.zeros((heads_here, tok_rows), jnp.float32),
-        jnp.zeros((heads_here, tok_rows, VDIM), jnp.float32),
+    updated = attention(
+        residual, query_nope, query_rope, kv_latent, rope_key, latent_gain, w_key, w_value, w_out, post_gain
     )
-    pieces = side_by_side((kv_latent, rope_key), SP, 0, 1)
-
-    def take_piece(state_in):
-        key_plain, value_plain, key_turned = expand(
-            pieces[0], pieces[1], latent_gain, w_key, w_value
-        )
-        return update(state_in, key_plain, value_plain, key_turned)
-
-    def skip_piece(state_in):
-        return state_in
-
-    final_state = lax.cond(jnp.int32(0) <= last_row, take_piece, skip_piece, start_state)
-    attended = (final_state[2] / final_state[1][..., None]).transpose(1, 0, 2)
-    attended = attended.reshape(tok_rows, heads_here * VDIM).astype(jnp.bfloat16)
-    chosen = attended
-    product = jnp.dot(chosen, w_out, preferred_element_type=jnp.float32)
-    branch = summed_on_arrival(
-        product.astype(jnp.bfloat16).astype(jnp.float32).astype(jnp.bfloat16), "tp", 0
-    )
-    updated = (residual.astype(jnp.float32) + rms_scale(branch, post_gain)).astype(jnp.bfloat16)
     return moe(updated, routes, route_weight, moe_gain, w_gate, w_up, w_down)
 
 

time: 300 us -> 192 us (0.64)
  waiting for transfers between devices: 108 us -> 0 us
  Pallas kernels: 111 us -> 182 us
  matrix products: 31.1 us -> 0 us
  other arithmetic: 21.1 us -> 1.52 us
  between operations: 13.5 us -> 0.04 us
  starting transfers between devices: 4.23 us -> 0 us
  local copies, waits for them, and re-layouts: 8.37 us -> 4.56 us
    all_gather x1 -> x0, waiting for transfers between devices: 94.3 us -> none  [side_by_side(): result = lax.all_gather(both, axis, axis=dim, tiled=True)]
    pallas_call x0 -> x1, Pallas kernels: none -> 70.3 us  [attention(): pl.pallas_call(functools.partial(attention_kernel, n_sp, n_tp, heads), ou...]
    dot_general x5 -> x0, matrix products: 28 us -> none  [the longest x1 11 us: update(): jnp.einsum('thd,sd->hts', query_turned, key_turned, preferred_element_typ...]
    all_to_all x1 -> x0, waiting for transfers between devices: 14.1 us -> none  [summed_on_arrival(): lax.all_to_all(split_up(array, dim, length), axis, 0, 0, tiled=True)]
    reduce_sum x4 -> x0, other arithmetic: 11.3 us -> none  [the longest x1 7.96 us: update(): row_sum = jnp.sum(weights, axis=-1)]
    another operation x3 -> x0, other arithmetic: 4.41 us -> none
    all_to_all x1 -> x0, starting transfers between devices: 4.23 us -> none  [summed_on_arrival(): lax.all_to_all(split_up(array, dim, length), axis, 0, 0, tiled=True)]
    cond x8 -> x0, local copies, waits for them, and re-layouts: 3.26 us -> none
  transfers between devices with their start and end apart: 2 -> 0, of which waited for: 2 -> 0; matrix products, arithmetic and copies ran while one was open for 1% -> 0% of each run, Pallas kernels for 0% -> 0%
where the time goes in v2:
time: 192 us; the launch traced here: 189 us
  Pallas kernels  182 us (95%)
  local copies, waits for them, and re-layouts  4.56 us (2%)
    pallas_call x1, Pallas kernels, moe(): pl.pallas_call(functools.partial(moe_kernel, n_sp, n_tp, cap), out_shape=...  112 us
    pallas_call x1, Pallas kernels, attention(): pl.pallas_call(functools.partial(attention_kernel, n_sp, n_tp, heads), ou...  70.3 us
    unnamed x8, local copies, waits for them, and re-layouts  4.56 us

profile of v2, /device:TPU:40, one launch (start us, length us, event | category | flops | bytes accessed | tf_op | source)
XLA Modules:
  0.0 188.5 jit_solution(2355035755099536010)
XLA Ops:
  0.0 0.0 copy-start
  0.0 0.0 copy-start.1
  0.0 0.5 fusion
  0.6 1.0 pad_maximum_fusion
  1.5 1.5 copy.23.rope_key_ref
  3.0 70.3 %shard_map.172.updated_ref = bf16[64,2048]{1,0:T(8,128)(2,1)} custom-call(bf16[64,2048]{1,0:T(8,128)(2,1)} %residual_ref.1, bf16[256,256]{1,0:T(8,128)(2,1)} %nope_ref.1, bf16[256,128]{1,0:T(8,128)(2,1)} %rope_ref.1, bf16[256,256]{1,0:T(8,128)(2,1)} %latent_ref.1, bf16[256,64]{1,0:T(8,128)(2,1)} %copy.23.rope_key_ref, f32[1,256]{1,0:T(1,128)} %bitcast.5, ...), custom_call_target="tpu_custom_call" | custom-call | tf_op jit(solution)/shard_map/pallas_call | solution.py:596
  73.4 0.0 copy-done
  73.4 0.7 copy.24.routes_ref
  74.1 0.0 copy-done.1
  74.1 0.7 copy.25.weight_ref
  74.8 112.1 %shard_map.173 = bf16[64,2048]{1,0:T(8,128)(2,1)} custom-call(bf16[64,2048]{1,0:T(8,128)(2,1)} %shard_map.172.updated_ref, s32[64,2]{1,0:T(8,128)} %copy.24.routes_ref, f32[64,2]{1,0:T(8,128)} %copy.25.weight_ref, f32[1,2048]{1,0:T(1,128)} %bitcast.4, bf16[192,192]{1,0:T(8,128)(2,1)} %constant.20.clone.fold_ref, bf16[192,192]{1,0:T(8,128)(2,1)} %constant.21.clone.unfold_ref, ...), custom_call_target="tpu_custom_call" | custom-call | tf_op jit(solution)/shard_map/pallas_call | solution.py:304
  186.9 1.7 copy.27
  (2 shorter events, 0.0 us)
Async XLA Ops:
  0.0 73.4 %copy-start = (s32[64,2]{0,1:T(2,128)S(1)}, s32[64,2]{0,1:T(2,128)}, u32[]{:S(2)}) copy-start(s32[64,2]{0,1:T(2,128)} %param.28) | copy-start | bytes 1540
  0.0 74.1 %copy-start.1 = (f32[64,2]{0,1:T(2,128)S(1)}, f32[64,2]{0,1:T(2,128)}, u32[]{:S(2)}) copy-start(f32[64,2]{0,1:T(2,128)} %param.29) | copy-start | bytes 1540
